TPU v7x, 128 devices: a whole 4x4x4 slice. The times are simulated.
128 devices in a mesh: sp: 32 (over z, y, core), tp: 4 (over x).
Axes of the slice: x: 4, y: 4, z: 4, core: 2. Of those that a mesh axis runs over, the one named last changes fastest.
Arguments:
- queries: bfloat16 [12288, 1024], P('sp', 'tp'), may hold values from -10 to 10
- key_rows: bfloat16 [12288, 256], P('sp', 'tp'), may hold values from -10 to 10
- value_rows: bfloat16 [12288, 256], P('sp', 'tp'), may hold values from -6 to 6
- key_logit: bfloat16 [12288, 4], P('sp', 'tp'), may hold values from -3 to 17
- head_offset: float32 [16], P('tp'), may hold values from -17.5 to -4
- stream: bfloat16 [12288, 2048], P(('sp', 'tp')), may hold values from -3 to 3
- out_weight: bfloat16 [1024, 2048], replicated, may hold values from -0.1875 to 0.1875
- norm_gain: float32 [2048], replicated, may hold values from 0.1 to 1.9
- expert_ids: int32 [12288, 2], P(('sp', 'tp')), may hold values from 0 to 127, as said below
- group_logit: float32 [12288], P(('sp', 'tp')), may hold values from -6 to 6
- expert_logits: float32 [12288, 2], P(('sp', 'tp')), may hold values from -6 to 6
- gate_weight: bfloat16 [128, 2048, 1024], P(('sp', 'tp')), may hold values from -0.125 to 0.125
- up_weight: bfloat16 [128, 2048, 1024], P(('sp', 'tp')), may hold values from -0.125 to 0.125
- down_weight: bfloat16 [128, 1024, 2048], P(('sp', 'tp')), may hold values from -0.1875 to 0.1875
Outputs:
- result: bfloat16 [12288, 2048], P(('sp', 'tp'))
Inputs may be any that keep to these rules, and one draw needn't show every extreme that they name: `expert_ids`: the two numbers of a row differ and lie in one group of 4 consecutive numbers. In the rows of one device (aligned blocks of 96 rows) no number is named more than 3 times, and in every block some number is named exactly 3 times.
All inputs are finite; a program needn't handle non-finite values.
Results may differ from a plain program's by a relative error of at most 0.012.
Values may be sent and summed in bfloat16 or wider, within the bound.
A program may use at most 128 MiB of HBM per device.

v0:
```python
import jax
import jax.numpy as jnp
from jax import lax
from jax.sharding import PartitionSpec as P

HEAD_DIM = 64
GROUP_EXPERTS = 4
TOP = 2


norm_eps = 1e-06


def sent_together(arrays, axis, dim, along):
    both = jnp.concatenate(arrays, axis=along)
    result, at, done = (lax.all_gather(both, axis, axis=dim, tiled=True), 0, [])
    for a in arrays:
        done.append(lax.slice_in_dim(result, at, at + a.shape[along], axis=along))
        at += a.shape[along]
    return tuple(done)


def shard_terms(query_heads, offsets, key_piece, value_piece, logit_piece, carried, causal):
    key_count = key_piece.shape[0]
    heads_here = offsets.shape[0]
    key_heads = key_piece.reshape(key_count, heads_here, HEAD_DIM)
    value_heads = value_piece.reshape(key_count, heads_here, HEAD_DIM)
    scores = jnp.einsum(
        "qcgd,kcd->cgqk", query_heads, key_heads, preferred_element_type=jnp.float32
    ) * HEAD_DIM ** (-0.5)
    scores = (
        scores + offsets[:, :, None, None] + logit_piece.astype(jnp.float32).T[:, None, None, :]
    )
    stay_log = jax.nn.log_sigmoid(-scores)
    if causal:
        query_count = query_heads.shape[0]
        allowed = jnp.arange(key_count)[None, :] < jnp.arange(query_count)[:, None]
        keep_log = jnp.where(allowed, stay_log, 0.0)
    else:
        keep_log = stay_log
    later_log = jnp.concatenate([keep_log[..., 1:], jnp.zeros_like(keep_log[..., :1])], axis=3)
    survive = lax.cumsum(later_log, axis=3, reverse=True)
    log_weight = scores + stay_log + survive + carried[..., None]
    if causal:
        weight = jnp.where(allowed, jnp.exp(log_weight), 0.0)
    else:
        weight = jnp.exp(log_weight)
    weight = weight.astype(jnp.bfloat16)
    added = jnp.einsum("cgqk,kcd->qcgd", weight, value_heads, preferred_element_type=jnp.float32)
    return (added, carried + jnp.sum(keep_log, axis=3))


def expert_apply(incoming, gate_one, up_one, down_one):
    flat_rows = incoming.reshape(-1, incoming.shape[-1])
    gate_act = jnp.dot(flat_rows, gate_one, preferred_element_type=jnp.float32)
    upward = jnp.dot(flat_rows, up_one, preferred_element_type=jnp.float32)
    hidden = (jax.nn.silu(gate_act) * upward).astype(jnp.bfloat16)
    produced = jnp.dot(hidden, down_one, preferred_element_type=jnp.float32).astype(jnp.bfloat16)
    return produced.reshape(incoming.shape)


def on_device(
    queries,
    key_rows,
    value_rows,
    key_logit,
    head_offset,
    stream,
    out_weight,
    norm_gain,
    expert_ids,
    group_logit,
    expert_logits,
    gate_weight,
    up_weight,
    down_weight,
):
    rows_here = queries.shape[0]
    heads_here = key_rows.shape[1] // HEAD_DIM
    group_share = queries.shape[1] // HEAD_DIM // heads_here
    query_heads = queries.reshape(rows_here, heads_here, group_share, HEAD_DIM)
    offsets = head_offset.reshape(heads_here, group_share)
    start_carry = jnp.zeros((heads_here, group_share, rows_here), jnp.float32)
    own_added, own_carry = shard_terms(
        query_heads, offsets, key_rows, value_rows, key_logit, start_carry, True
    )
    position = lax.axis_index("sp")
    whole_keys, whole_values, whole_logits = sent_together(
        (key_rows, value_rows, key_logit), "sp", 0, 1
    )

    def gathered_step(step_index, loop_state):
        summed, carried = loop_state
        first_row = (position - step_index) * rows_here
        key_piece = lax.dynamic_slice_in_dim(whole_keys, first_row, rows_here, 0)
        value_piece = lax.dynamic_slice_in_dim(whole_values, first_row, rows_here, 0)
        logit_piece = lax.dynamic_slice_in_dim(whole_logits, first_row, rows_here, 0)
        added, carried = shard_terms(
            query_heads, offsets, key_piece, value_piece, logit_piece, carried, False
        )
        return (summed + added, carried)

    summed, carried = lax.fori_loop(1, position + 1, gathered_step, (own_added, own_carry))
    attended = summed.reshape(rows_here, -1).astype(jnp.bfloat16)
    token_heads = lax.all_to_all(attended, "tp", split_axis=0, concat_axis=1, tiled=True)
    mixed_rows = (
        stream.astype(jnp.float32)
        + jnp.dot(token_heads, out_weight, preferred_element_type=jnp.float32)
    ).astype(jnp.bfloat16)
    mixed_wide = mixed_rows.astype(jnp.float32)
    normed = (
        mixed_wide
        * lax.rsqrt(jnp.mean(mixed_wide * mixed_wide, axis=-1, keepdims=True) + norm_eps)
        * norm_gain
    ).astype(jnp.bfloat16)
    expert_exp = jnp.exp(expert_logits)
    route_weight = (
        jax.nn.sigmoid(group_logit)[:, None]
        * expert_exp
        / jnp.sum(expert_exp, axis=1, keepdims=True)
    )
    rows_count = stream.shape[0]
    expert_total = gate_weight.shape[0] * lax.axis_size("sp") * lax.axis_size("tp")
    capacity = rows_count * GROUP_EXPERTS // expert_total
    flat_ids = expert_ids.reshape(-1)
    matches = (flat_ids[:, None] == jnp.arange(expert_total, dtype=jnp.int32)[None, :]).astype(
        jnp.int32
    )
    ranking = jnp.sum(jnp.cumsum(matches, axis=0) * matches, axis=1) - 1
    slot_index = flat_ids * capacity + ranking
    chooser = jnp.arange(expert_total * capacity, dtype=jnp.int32)[:, None] == slot_index[None, :]
    chooser = jnp.sum(
        chooser.reshape(expert_total * capacity, rows_count, TOP).astype(jnp.int32), axis=2
    ).astype(jnp.bfloat16)
    outgoing = jnp.dot(chooser, normed, preferred_element_type=jnp.float32).astype(jnp.bfloat16)
    outgoing = outgoing.reshape(expert_total, capacity, -1)
    produced = expert_apply(
        lax.all_to_all(outgoing, ("sp", "tp"), split_axis=0, concat_axis=0, tiled=True),
        gate_weight[0],
        up_weight[0],
        down_weight[0],
    )
    returned = lax.all_to_all(produced, ("sp", "tp"), split_axis=0, concat_axis=0, tiled=True)
    back_rows = returned.reshape(expert_total * capacity, -1)
    picked = (
        jnp.take(back_rows, slot_index, axis=0).reshape(rows_count, TOP, -1).astype(jnp.float32)
    )
    combined = mixed_wide + jnp.sum(route_weight[:, :, None] * picked, axis=1)
    return combined.astype(jnp.bfloat16)


def solution(mesh):
    placed = (
        P("sp", "tp"),
        P("sp", "tp"),
        P("sp", "tp"),
        P("sp", "tp"),
        P("tp"),
        P(("sp", "tp"), None),
        P(),
        P(),
        P(("sp", "tp"), None),
        P(("sp", "tp")),
        P(("sp", "tp"), None),
        P(("sp", "tp"), None, None),
        P(("sp", "tp"), None, None),
        P(("sp", "tp"), None, None),
    )
    return jax.shard_map(
        on_device, mesh=mesh, in_specs=placed, out_specs=P(("sp", "tp"), None), check_vma=False
    )
```

profile of v0, /device:TPU:1, one launch (start us, length us, event | category | flops | bytes accessed | tf_op | source)
XLA Modules:
  0.0 947.1 jit_solution(6434160528991273907)
XLA Ops:
  6.5 1.5 pad_maximum_fusion
  8.1 1.1 copy.74
  9.2 0.7 convert_reduce_fusion.2
  9.9 4.2 fusion.65
  14.4 14.3 %fusion.29 = f32[1,4,384,3,128]{2,3,4,1,0:T(4,128)S(1)} fusion(f32[1,4,384,3,128]{2,4,3,1,0:T(8,128)S(1)} %bitcast.222), kind=kOutput, calls=%fused_computation.42 | output fusion | flops 74907648 | bytes 4718592 | tf_op jit(solution)/shard_map/reduce-window.2
  30.4 4.0 fusion.38
  34.8 25.4 %all-gather.2.cloned.1.call-done = bf16[12288,129]{0,1:T(8,128)(2,1)} async-done(((bf16[384,129]{0,1:T(8,128)(2,1)}), bf16[12288,129]{0,1:T(8,128)(2,1)}) %all-gather.2.cloned.1.call-update) | async-done | bytes 3170320 | tf_op jit(solution)/shard_map/all_gather | solution.py:16
  60.2 3.8 fusion.67
  64.0 1.0 slice.55
  65.0 37.6 %while.12 = (s32[]{:T(128)}, f32[384,1,4,64]{0,3,2,1:T(8,128)S(1)}, f32[1,4,384]{2,1,0:T(4,128)S(1)}, s32[]{:T(128)}, s32[]{:T(128)}, /*index=5*/bf16[12288,64]{...) while((s32[]{:T(128)}, f32[384,1,4,64]{0,3,2,1:T(8,128)S(1)}, ...), condition=%wide.region_7.8_spmd, body=%wide.region_3.7_spmd.sunk | while | flops 241350528 | bytes 31905276 | solution.py:103
  78.6 4.0 fusion.83
  82.9 14.0 %fusion.84 = f32[1,4,384,3,128]{2,3,4,1,0:T(4,128)S(1)} fusion(f32[1,4,384,3,128]{2,4,3,1,0:T(8,128)S(1)} %bitcast.221), kind=kOutput, calls=%fused_computation.2.clone.1 | output fusion | flops 74907648 | bytes 4718592 | tf_op jit(solution)/shard_map/reduce-window
  97.3 4.0 fusion.85
  101.2 1.1 fusion.86
  102.9 0.8 copy.79
  103.7 4.0 all-to-all-start
  107.8 5.1 all-to-all-done
  112.9 3.1 multiply_reduce_fusion.1
  116.0 1.8 convolution_convert_fusion
  117.8 4.0 reshape.257
  121.8 749.7 %all_to_all.26 = bf16[128,3,2048]{2,1,0:T(4,128)(2,1)} all-to-all(bf16[128,3,2048]{2,1,0:T(4,128)(2,1)S(1)} %reshape.257), channel_id=1, replica_groups=mesh['sp'=32,'tp'=4] {'sp','tp'}, dimensions={0} | all-to-all | bytes 3145728 | tf_op jit(solution)/shard_map/all_to_all | solution.py:138
  871.5 3.9 reshape.258
  875.4 5.1 fusion.27
  880.6 8.6 fusion.31
  889.1 5.1 reshape.259
  894.3 5.4 all-to-all-start.2
  900.3 29.8 %all-to-all-done.2 = bf16[128,3,2048]{2,1,0:T(4,128)(2,1)} async-done(((bf16[128,3,2048]{2,1,0:T(4,128)(2,1)}), bf16[128,3,2048]{2,1,0:T(4,128)(2,1)}, u32[]{:S(2)}, u32[]{:S(2)}) %all-to-all-start.2) | async-done | bytes 1572896 | tf_op jit(solution)/shard_map/all_to_all | solution.py:143
  930.0 3.9 reshape.260
  934.0 1.1 gather_fusion
  935.1 0.5 gather.7
  935.6 3.3 multiply_reduce_fusion
  938.9 0.9 add_convert_fusion
  (63 shorter events, 3.9 us)
Async XLA Ops:
  6.5 53.7 %all-gather.2.cloned.1.call-start = ((), (), s32[]{:S(2)}) async-start(), calls=%async_computation.3 | async-start | bytes 3446784 | tf_op jit(solution)/shard_map/all_gather | solution.py:16
  28.7 0.7 copy-start.3
  28.7 1.7 copy-start.2
  30.4 4.0 copy-start.1
  102.6 10.2 %copy-start = (bf16[96,2048]{1,0:T(8,128)(2,1)S(1)}, bf16[96,2048]{1,0:T(8,128)(2,1)}, u32[]{:S(2)}) copy-start(bf16[96,2048]{1,0:T(8,128)(2,1)} %param.21) | copy-start | bytes 1179652
  103.7 9.1 all-to-all-start
  112.9 3.2 copy-start.4
  894.3 5.8 copy-start.5
  894.3 5.8 copy-start.6
  894.3 35.8 %all-to-all-start.2 = ((bf16[128,3,2048]{2,1,0:T(4,128)(2,1)}), bf16[128,3,2048]{2,1,0:T(4,128)(2,1)}, u32[]{:S(2)}, u32[]{:S(2)}) async-start(bf16[128,3,2048]{2,1,0:T(4,128)(2,1)} %reshape.259), calls=%async_computation.2 | async-start | bytes 4194304 | tf_op jit(solution)/shard_map/all_to_all | solution.py:143
Sparse Core Ops, SparseCore 0:
  9.5 50.6 all-gather.1
where the time goes:
time: 961 us; the launch traced here: 947 us
  blocking collectives  750 us (78%)
  waiting for transfers between devices  60.3 us (6%)
  other arithmetic  43.5 us (5%)
  matrix products  28.2 us (3%)
  local copies, waits for them, and re-layouts  28 us (3%)
  between operations  14.2 us (1%)
  loops' own time  13.9 us (1%)
    all_to_all x1, blocking collectives, on_device(): lax.all_to_all(outgoing, ('sp', 'tp'), split_axis=0, concat_axis=0, tiled...  750 us
    all_to_all x1, waiting for transfers between devices, on_device(): lax.all_to_all(produced, ('sp', 'tp'), split_axis=0, concat_axis=0, tiled...  29.8 us
    another operation x8, other arithmetic  28.6 us
    all_gather x1, waiting for transfers between devices, sent_together(): result, at, done = (lax.all_gather(both, axis, axis=dim, tiled=True), 0, [])  25.4 us
  transfers between devices with their start and end apart: 3, of which 3 were waited for; matrix products, arithmetic and copies ran while one was open for 3% of the time, Pallas kernels for 0%

commit v1 on v0

v1 whole, which is shorter than its diff:
```python
import functools
import jax
import jax.numpy as jnp
from jax import lax
from jax.experimental import pallas as pl
from jax.experimental.pallas import tpu as pltpu
from jax.sharding import PartitionSpec as P

HEAD_DIM = 64
GROUP_EXPERTS = 4
TOP = 2


norm_eps = 1e-06


HEADS = 4
BLK = 384
HALF = 192
SEG = 48
CHUNK = 16
COLS = 768
TILE = 256
LOG2E = 1.4426950408889634


def split3(x):
    hi = x.astype(jnp.bfloat16).astype(jnp.float32)
    rest = x - hi
    mid = rest.astype(jnp.bfloat16).astype(jnp.float32)
    lo = (rest - mid).astype(jnp.bfloat16).astype(jnp.float32)
    return hi, mid, lo


def attention_kernel(n, pos_ref, kv_ref, q_ref, off_ref, out_ref, qt, lk, vt, acc, carry, okay, wts):
    i = pos_ref[0]
    f32, bf16 = jnp.float32, jnp.bfloat16
    for s in range(2):
        qs = q_ref[s * HALF:(s + 1) * HALF, :].astype(f32) * (LOG2E * HEAD_DIM ** -0.5)
        rows = jnp.concatenate([qs[:, h * 64:(h + 1) * 64] for h in range(HEADS)], axis=0)
        high = rows.astype(bf16).astype(f32)
        low = rows - high
        zero = jnp.zeros_like(rows)
        top = jnp.concatenate([high, zero], axis=1).T
        bottom = jnp.concatenate([zero, low], axis=1).T
        lane = lax.broadcasted_iota(jnp.int32, (8, COLS), 1)
        off = jnp.zeros((8, COLS), f32)
        for h in range(HEADS):
            inside = jnp.logical_and(lane >= h * HALF, lane < (h + 1) * HALF)
            off = jnp.where(inside, off_ref[h] * LOG2E, off)
        hi, mid, lo = split3(off)
        row = lax.broadcasted_iota(jnp.int32, (8, COLS), 0)
        c_hi = 1.4453125
        extra = jnp.where(row == 0, c_hi, jnp.where(row == 1, LOG2E - c_hi, jnp.where(row == 2, hi, jnp.where(row == 3, mid, jnp.where(row == 4, lo, 0.0)))))
        bottom = jnp.concatenate([extra, bottom[8:, :]], axis=0)
        qt[0:128, s * COLS:(s + 1) * COLS] = top.astype(bf16)
        qt[128:256, s * COLS:(s + 1) * COLS] = bottom.astype(bf16)

    sub = lax.broadcasted_iota(jnp.int32, (8, TILE), 0)

    def exclusive(p):
        e = jnp.where(sub == 7, 1.0, pltpu.roll(p, 7, 0))
        e = e * jnp.where(sub == 7, 1.0, pltpu.roll(e, 7, 0))
        e = e * jnp.where(sub >= 6, 1.0, pltpu.roll(e, 6, 0))
        e = e * jnp.where(sub >= 4, 1.0, pltpu.roll(e, 4, 0))
        return e

    def tile(base, at, is_a, diag, slow):
        col = pl.multiple_of(base + at, 128)
        here = pl.ds(col, TILE)
        z = jnp.dot(lk[...], qt[:, here], preferred_element_type=f32)
        if diag:
            lane = lax.broadcasted_iota(jnp.int32, (8, TILE), 1)
            query = (lane + at) % HALF + jnp.where(is_a, 0, HALF)
            limit = query - sub * SEG
        start = carry[:, here]
        if slow:
            p = jnp.ones((8, TILE), f32)
            for r in reversed(range(SEG)):
                beta = 1.0 / (1.0 + jnp.exp2(-z[r * 8:(r + 1) * 8, :]))
                if diag:
                    beta = jnp.where(r < limit, beta, 0.0)
                w = p * beta
                p = p - w
                wts[r * 8:(r + 1) * 8, :] = w
            e = exclusive(p)
            total = e[0:1, :] * p[0:1, :]
            e = e * start
            scales = [e] * (SEG // CHUNK)
        else:
            ends, good = [], None
            for ch in range(SEG // CHUNK):
                f = jnp.ones((8, TILE), f32)
                for r in range(ch * CHUNK, (ch + 1) * CHUNK):
                    x = jnp.exp2(z[r * 8:(r + 1) * 8, :])
                    if diag:
                        x = jnp.where(r < limit, x, 0.0)
                    w = x * f
                    f = f + w
                    wts[r * 8:(r + 1) * 8, :] = w
                fine = jnp.where(f < 1e36, 1.0, 0.0)
                good = fine if good is None else jnp.minimum(good, fine)
                ends.append(1.0 / f)
            okay[:, 0:TILE] = jnp.minimum(okay[:, 0:TILE], good)
            p = ends[0] * ends[1] * ends[2]
            e = exclusive(p)
            total = e[0:1, :] * p[0:1, :]
            e = e * start
            s2 = e * ends[2]
            s1 = s2 * ends[1]
            scales = [s1 * ends[0], s1, s2]
        carry[:, here] = start * total
        both = [jnp.concatenate([s, s], axis=0) for s in scales]
        parts = []
        for r in range(0, SEG, 2):
            parts.append((wts[r * 8:(r + 2) * 8, :] * both[r // CHUNK]).astype(bf16))
        weight = jnp.concatenate(parts, axis=0)
        acc[:, here] += jnp.dot(vt[...], weight, preferred_element_type=f32)

    def sweep(slow):
        acc[...] = jnp.zeros_like(acc)
        carry[...] = jnp.ones_like(carry)

        def step(s, c):
            is_a = s <= i
            block = jnp.where(is_a, i - s, n - s)
            base = jnp.where(is_a, 0, COLS)
            rows = kv_ref[block, 0:BLK, :]
            lk[:, 0:128] = rows
            wide = rows.astype(f32)
            turned = pltpu.roll(wide, 64, 1)
            logit = kv_ref[block, BLK:BLK + 8, :].astype(f32)
            lane = lax.broadcasted_iota(jnp.int32, (128, 128), 1)
            for j in range(3):
                column = jnp.broadcast_to(logit[j:j + 1, :], (128, 128)).T
                side = jnp.where(lane < 2, column, jnp.where(lane < 5, 1.0, jnp.where(lane < 64, 0.0, turned[j * 128:(j + 1) * 128, :])))
                lk[j * 128:(j + 1) * 128, 128:256] = side.astype(bf16)
            vt[...] = wide.T[64:128, :].astype(bf16)
            edge = jnp.logical_or(s == 0, s == i + 1)

            @pl.when(edge)
            def _():
                for at in range(0, COLS, TILE):
                    tile(base, at, is_a, True, slow)

            @pl.when(jnp.logical_not(edge))
            def _():
                for at in range(0, COLS, TILE):
                    tile(base, at, is_a, False, slow)
            return c

        lax.fori_loop(0, n + 1, step, 0)

    okay[...] = jnp.ones_like(okay)
    sweep(False)

    @pl.when(jnp.min(okay[...]) < 0.5)
    def _():
        sweep(True)

    stacked = jnp.concatenate([acc[:, 0:COLS], acc[:, COLS:2 * COLS]], axis=0).T
    for s in range(2):
        heads = [stacked[h * HALF:(h + 1) * HALF, s * 64:(s + 1) * 64] for h in range(HEADS)]
        out_ref[s * HALF:(s + 1) * HALF, :] = jnp.concatenate(heads, axis=1).astype(bf16)


def attention(n, position, kv, q, offsets):
    vm = pl.BlockSpec(memory_space=pltpu.VMEM)
    sm = pl.BlockSpec(memory_space=pltpu.SMEM)
    return pl.pallas_call(
        functools.partial(attention_kernel, n),
        out_shape=jax.ShapeDtypeStruct((BLK, HEADS * HEAD_DIM), jnp.bfloat16),
        in_specs=[sm, vm, vm, sm],
        out_specs=vm,
        scratch_shapes=[
            pltpu.VMEM((256, 2 * COLS), jnp.bfloat16),
            pltpu.VMEM((BLK, 256), jnp.bfloat16),
            pltpu.VMEM((64, BLK), jnp.bfloat16),
            pltpu.VMEM((64, 2 * COLS), jnp.float32),
            pltpu.VMEM((8, 2 * COLS), jnp.float32),
            pltpu.VMEM((8, TILE), jnp.float32),
            pltpu.VMEM((BLK, TILE), jnp.float32),
        ],
        compiler_params=pltpu.CompilerParams(vmem_limit_bytes=40 * 1024 * 1024),
        name="attention",
    )(position, kv, q, offsets)


def pack_block(key_rows, value_rows, key_logit):
    both = jnp.concatenate([key_rows, value_rows], axis=1)
    both = both.reshape(8, SEG, 128).transpose(1, 0, 2).reshape(BLK, 128)
    logit = key_logit.reshape(8, SEG).T.reshape(3, 128)
    return jnp.concatenate([both, logit, jnp.zeros((13, 128), jnp.bfloat16)], axis=0)


def expert_apply(incoming, gate_one, up_one, down_one):
    flat_rows = incoming.reshape(-1, incoming.shape[-1])
    gate_act = jnp.dot(flat_rows, gate_one, preferred_element_type=jnp.float32)
    upward = jnp.dot(flat_rows, up_one, preferred_element_type=jnp.float32)
    hidden = (jax.nn.silu(gate_act) * upward).astype(jnp.bfloat16)
    produced = jnp.dot(hidden, down_one, preferred_element_type=jnp.float32).astype(jnp.bfloat16)
    return produced.reshape(incoming.shape)


def on_device(
    queries,
    key_rows,
    value_rows,
    key_logit,
    head_offset,
    stream,
    out_weight,
    norm_gain,
    expert_ids,
    group_logit,
    expert_logits,
    gate_weight,
    up_weight,
    down_weight,
):
    n = lax.axis_size("sp")
    position = lax.axis_index("sp").astype(jnp.int32).reshape(1)
    mirror = [(a, n - 1 - a) for a in range(n)]
    block = pack_block(key_rows, value_rows, key_logit)
    kv = lax.all_gather(block, "sp", axis=0)
    late = lax.ppermute(queries[HALF:], "sp", mirror)
    halves = attention(n, position, kv, jnp.concatenate([queries[:HALF], late], axis=0), head_offset)
    attended = jnp.concatenate([halves[:HALF], lax.ppermute(halves[HALF:], "sp", mirror)], axis=0)
    token_heads = lax.all_to_all(attended, "tp", split_axis=0, concat_axis=1, tiled=True)
    mixed_rows = (
        stream.astype(jnp.float32)
        + jnp.dot(token_heads, out_weight, preferred_element_type=jnp.float32)
    ).astype(jnp.bfloat16)
    mixed_wide = mixed_rows.astype(jnp.float32)
    normed = (
        mixed_wide
        * lax.rsqrt(jnp.mean(mixed_wide * mixed_wide, axis=-1, keepdims=True) + norm_eps)
        * norm_gain
    ).astype(jnp.bfloat16)
    expert_exp = jnp.exp(expert_logits)
    route_weight = (
        jax.nn.sigmoid(group_logit)[:, None]
        * expert_exp
        / jnp.sum(expert_exp, axis=1, keepdims=True)
    )
    rows_count = stream.shape[0]
    expert_total = gate_weight.shape[0] * lax.axis_size("sp") * lax.axis_size("tp")
    capacity = rows_count * GROUP_EXPERTS // expert_total
    flat_ids = expert_ids.reshape(-1)
    matches = (flat_ids[:, None] == jnp.arange(expert_total, dtype=jnp.int32)[None, :]).astype(
        jnp.int32
    )
    ranking = jnp.sum(jnp.cumsum(matches, axis=0) * matches, axis=1) - 1
    slot_index = flat_ids * capacity + ranking
    chooser = jnp.arange(expert_total * capacity, dtype=jnp.int32)[:, None] == slot_index[None, :]
    chooser = jnp.sum(
        chooser.reshape(expert_total * capacity, rows_count, TOP).astype(jnp.int32), axis=2
    ).astype(jnp.bfloat16)
    outgoing = jnp.dot(chooser, normed, preferred_element_type=jnp.float32).astype(jnp.bfloat16)
    outgoing = outgoing.reshape(expert_total, capacity, -1)
    produced = expert_apply(
        lax.all_to_all(outgoing, ("sp", "tp"), split_axis=0, concat_axis=0, tiled=True),
        gate_weight[0],
        up_weight[0],
        down_weight[0],
    )
    returned = lax.all_to_all(produced, ("sp", "tp"), split_axis=0, concat_axis=0, tiled=True)
    back_rows = returned.reshape(expert_total * capacity, -1)
    picked = (
        jnp.take(back_rows, slot_index, axis=0).reshape(rows_count, TOP, -1).astype(jnp.float32)
    )
    combined = mixed_wide + jnp.sum(route_weight[:, :, None] * picked, axis=1)
    return combined.astype(jnp.bfloat16)


def solution(mesh):
    placed = (
        P("sp", "tp"),
        P("sp", "tp"),
        P("sp", "tp"),
        P("sp", "tp"),
        P("tp"),
        P(("sp", "tp"), None),
        P(),
        P(),
        P(("sp", "tp"), None),
        P(("sp", "tp")),
        P(("sp", "tp"), None),
        P(("sp", "tp"), None, None),
        P(("sp", "tp"), None, None),
        P(("sp", "tp"), None, None),
    )
    return jax.shard_map(
        on_device, mesh=mesh, in_specs=placed, out_specs=P(("sp", "tp"), None), check_vma=False
    )
```

time: 961 us -> 245 us (0.25); the launches traced: 947 us -> 244 us
  blocking collectives: 750 us -> 36.4 us
  Pallas kernels: 0 us -> 44.3 us
  other arithmetic: 43.5 us -> 7.08 us
  waiting for transfers between devices: 60.3 us -> 79.2 us
  loops' own time: 13.9 us -> 0 us
  starting transfers between devices: 9.38 us -> 19.2 us
    all_to_all x1, blocking collectives: 750 us -> 36.4 us  [on_device(): lax.all_to_all(outgoing, ('sp', 'tp'), split_axis=0, concat_axis=0, tiled...]
    pallas_call x0 -> x1, Pallas kernels: none -> 44.3 us  [attention(): pl.pallas_call(functools.partial(attention_kernel, n), out_shape=jax.Shap...]
    another operation x8 -> x4, other arithmetic: 28.6 us -> 0.2 us
    another operation x1 -> x0, loops' own time: 13.9 us -> none  [on_device(): lax.fori_loop(1, position + 1, gathered_step, (own_added, own_carry))]
    all_gather x1, waiting for transfers between devices: 25.4 us -> 37.7 us  [on_device(): kv = lax.all_gather(block, 'sp', axis=0)]
    ppermute x0 -> x2, starting transfers between devices: none -> 10.2 us  [the longest x1 7.67 us: on_device(): late = lax.ppermute(queries[HALF:], 'sp', mirror)]
    dot_general x4 -> x0, matrix products: 9.62 us -> none  [the longest x2 8.15 us: shard_terms(): jnp.einsum('qcgd,kcd->cgqk', query_heads, key_heads, preferred_element_ty...]
  transfers between devices with their start and end apart: 3 -> 5, of which waited for: 3 -> 5; matrix products, arithmetic and copies ran while one was open for 3% -> 1% of each run, Pallas kernels for 0% -> 0%
where the time goes in v1:
time: 245 us; the launch traced here: 244 us
  waiting for transfers between devices  79.2 us (32%)
  Pallas kernels  44.3 us (18%)
  blocking collectives  36.4 us (15%)
  local copies, waits for them, and re-layouts  25.4 us (10%)
  starting transfers between devices  19.2 us (8%)
  matrix products  18.6 us (8%)
  between operations  13.7 us (6%)
  other arithmetic  7.08 us (3%)
    pallas_call x1, Pallas kernels, attention(): pl.pallas_call(functools.partial(attention_kernel, n), out_shape=jax.Shap...  44.3 us
    all_gather x1, waiting for transfers between devices, on_device(): kv = lax.all_gather(block, 'sp', axis=0)  37.7 us
    all_to_all x1, blocking collectives, on_device(): lax.all_to_all(outgoing, ('sp', 'tp'), split_axis=0, concat_axis=0, tiled...  36.4 us
    all_to_all x1, waiting for transfers between devices, on_device(): lax.all_to_all(produced, ('sp', 'tp'), split_axis=0, concat_axis=0, tiled...  30 us
    dot_general x1, matrix products, expert_apply(): jnp.dot(hidden, down_one, preferred_element_type=jnp.float32)  8.56 us
    ppermute x1, starting transfers between devices, on_device(): late = lax.ppermute(queries[HALF:], 'sp', mirror)  7.67 us
    ppermute x1, waiting for transfers between devices, on_device(): lax.ppermute(halves[HALF:], 'sp', mirror)  5.33 us
    reshape x1, local copies, waits for them, and re-layouts, expert_apply(): return produced.reshape(incoming.shape)  5.15 us
  transfers between devices with their start and end apart: 5, of which 5 were waited for; matrix products, arithmetic and copies ran while one was open for 1% of the time, Pallas kernels for 0%

profile of v1, /device:TPU:1, one launch (start us, length us, event | category | flops | bytes accessed | tf_op | source)
XLA Modules:
  0.0 243.9 jit_solution(15959334419206256108)
XLA Ops:
  6.5 0.9 copy.60
  7.5 0.9 copy.61
  8.5 0.7 reduce
  9.6 0.8 maximum_maximum_fusion
  10.4 1.0 fusion.26
  11.4 7.7 %collective-permute-start = (bf16[192,256]{1,0:T(8,128)(2,1)S(1)}, bf16[192,256]{1,0:T(8,128)(2,1)S(1)}, u32[]{:S(2)}, u32[]{:S(2)}) collective-permute-start(bf16[192,256]{1,0:T(8,128)(2,1)S(1)} %get-tuple-element.10), channel_id=1, source_target_pairs={{0,124},{4,120},{8,116},{12,112},{16,108},{20,104},{24,100},{28,96... | collective-permute-start | bytes 294920 | tf_op jit(solution)/shard_map/ppermute | solution.py:226
  19.0 0.8 copy.66
  20.3 0.2 fusion.20
  20.5 1.1 collective-permute-done
  21.7 37.7 %all-gather.3.cloned.1.call-done = bf16[12800,128]{1,0:T(8,128)(2,1)} async-done(((bf16[400,128]{1,0:T(8,128)(2,1)}), bf16[12800,128]{1,0:T(8,128)(2,1)}) %all-gather.3.cloned.1.call-update) | async-done | bytes 3276816 | tf_op jit(solution)/shard_map/all_gather | solution.py:225
  59.3 1.9 copy-done
  61.3 44.3 %attention.1 = bf16[384,256]{1,0:T(8,128)(2,1)S(1)} custom-call(s32[1]{0:T(128)} %bitcast.pos_ref, bf16[32,400,128]{2,1,0:T(8,128)(2,1)S(1)} %bitcast.43, bf16[384,256]{1,0:T(8,128)(2,1)S(1)} %pad_maximum_fusion.q_ref, f32[4]{0:T(128)S(1)} %copy-done.1), custom_call_target="tpu_custom_call" | custom-call | tf_op jit(solution)/shard_map/attention/pallas_call | solution.py:170
  105.6 2.6 %collective-permute-start.1 = (bf16[192,256]{1,0:T(8,128)(2,1)S(1)}, bf16[192,256]{1,0:T(8,128)(2,1)S(1)}, u32[]{:S(2)}, u32[]{:S(2)}) collective-permute-start(bf16[192,256]{1,0:T(8,128)(2,1)S(1)} %get-tuple-element.8), channel_id=1, source_target_pairs={{0,124},{4,120},{8,116},{12,112},{16,108},{20,104},{24,100},{28,96... | collective-permute-start | bytes 294920 | tf_op jit(solution)/shard_map/ppermute | solution.py:228
  108.4 5.3 %collective-permute-done.1 = bf16[192,256]{1,0:T(8,128)(2,1)S(1)} collective-permute-done((bf16[192,256]{1,0:T(8,128)(2,1)S(1)}, bf16[192,256]{1,0:T(8,128)(2,1)S(1)}, u32[]{:S(2)}, u32[]{:S(2)}) %collective-permute-start.1) | collective-permute-done | bytes 98336 | tf_op jit(solution)/shard_map/ppermute | solution.py:228
  113.7 0.7 pad_maximum_fusion.1
  114.4 4.0 %all-to-all-start = ((bf16[4,96,256]{2,1,0:T(8,128)(2,1)}), bf16[4,96,256]{2,1,0:T(8,128)(2,1)S(1)}, u32[]{:S(2)}, u32[]{:S(2)}) async-start(bf16[4,96,256]{2,1,0:T(8,128)(2,1)} %bitcast.6), calls=%async_computation | async-start | bytes 393216 | tf_op jit(solution)/shard_map/all_to_all | solution.py:229
  118.5 5.1 %all-to-all-done = bf16[4,96,256]{2,1,0:T(8,128)(2,1)S(1)} async-done(((bf16[4,96,256]{2,1,0:T(8,128)(2,1)}), bf16[4,96,256]{2,1,0:T(8,128)(2,1)S(1)}, u32[]{:S(2)}, u32[]{:S(2)}) %all-to-all-start) | async-done | bytes 196640 | tf_op jit(solution)/shard_map/all_to_all | solution.py:229
  123.6 3.1 %multiply_reduce_fusion.1 = (f32[96]{0:T(128)S(1)}, f32[96,2048]{1,0:T(8,128)S(1)}) fusion(bf16[96,1024]{1,0:T(8,128)(2,1)S(1)} %bitcast.44, bf16[1024,2048]{1,0:T(8,128)(2,1)} %param.20, bf16[96,2048]{1,0:T(8,128)(2,1)S(1)} %copy-done.2), kind=kOutput, calls=%fused_computation.18 | convolution fusion | flops 403832736 | bytes 5570944 | tf_op jit(solution)/shard_map/dot_general | solution.py:232
  126.8 1.8 convolution_convert_fusion
  128.6 4.0 %reshape.132 = bf16[128,3,2048]{2,1,0:T(4,128)(2,1)S(1)} reshape(bf16[384,2048]{1,0:T(8,128)(2,1)} %convolution_convert_fusion) | data formatting | bytes 3145728 | tf_op jit(solution)/shard_map/reshape | solution.py:260
  132.6 36.4 %all_to_all.29 = bf16[128,3,2048]{2,1,0:T(4,128)(2,1)} all-to-all(bf16[128,3,2048]{2,1,0:T(4,128)(2,1)S(1)} %reshape.132), channel_id=1, replica_groups=mesh['sp'=32,'tp'=4] {'sp','tp'}, dimensions={0} | all-to-all | bytes 3145728 | tf_op jit(solution)/shard_map/all_to_all | solution.py:262
  169.1 3.9 %reshape.133 = bf16[384,2048]{1,0:T(8,128)(2,1)S(1)} reshape(bf16[128,3,2048]{2,1,0:T(4,128)(2,1)} %all_to_all.29) | data formatting | bytes 3145728 | tf_op jit(solution)/shard_map/reshape | solution.py:197
  173.0 5.1 %fusion.4 = f32[384,1024]{1,0:T(8,128)} fusion(bf16[384,2048]{1,0:T(8,128)(2,1)S(1)} %reshape.133, bf16[1,2048,1024]{2,1,0:T(8,128)(2,1)} %param.25), kind=kOutput, calls=%fused_computation.5 | convolution fusion | flops 1610612736 | bytes 7340032 | tf_op jit(solution)/shard_map/dot_general | solution.py:198
  178.1 8.6 %fusion.6 = bf16[384,2048]{1,0:T(8,128)(2,1)} fusion(bf16[1,1024,2048]{2,1,0:T(8,128)(2,1)} %param.27, f32[384,1024]{1,0:T(8,128)} %fusion.4, bf16[384,2048]{1,0:T(8,128)(2,1)S(1)} %reshape.133, bf16[1,2048,1024]{2,1,0:T(8,128)(2,1)} %param.26), kind=kOutput, calls=%fused_computation.7 | convolution fusion | flops 3224371200 | bytes 13107200 | tf_op jit(solution)/shard_map/dot_general | solution.py:201
  186.7 5.1 %reshape.134 = bf16[128,3,2048]{2,1,0:T(4,128)(2,1)} reshape(bf16[384,2048]{1,0:T(8,128)(2,1)} %fusion.6) | data formatting | bytes 3145728 | tf_op jit(solution)/shard_map/reshape | solution.py:202
  191.8 5.0 %all-to-all-start.2 = ((bf16[128,3,2048]{2,1,0:T(4,128)(2,1)}), bf16[128,3,2048]{2,1,0:T(4,128)(2,1)}, u32[]{:S(2)}, u32[]{:S(2)}) async-start(bf16[128,3,2048]{2,1,0:T(4,128)(2,1)} %reshape.134), calls=%async_computation.2 | async-start | bytes 4194304 | tf_op jit(solution)/shard_map/all_to_all | solution.py:267
  197.4 30.0 %all-to-all-done.2 = bf16[128,3,2048]{2,1,0:T(4,128)(2,1)} async-done(((bf16[128,3,2048]{2,1,0:T(4,128)(2,1)}), bf16[128,3,2048]{2,1,0:T(4,128)(2,1)}, u32[]{:S(2)}, u32[]{:S(2)}) %all-to-all-start.2) | async-done | bytes 1572896 | tf_op jit(solution)/shard_map/all_to_all | solution.py:267
  227.3 3.9 %reshape.135 = bf16[384,2048]{1,0:T(8,128)(2,1)S(1)} reshape(bf16[128,3,2048]{2,1,0:T(4,128)(2,1)} %all-to-all-done.2) | data formatting | bytes 3145728 | tf_op jit(solution)/shard_map/reshape | solution.py:268
  231.3 1.1 gather_fusion
  232.4 0.5 gather.7
  232.9 3.3 %multiply_reduce_fusion = f32[96,2048]{1,0:T(8,128)S(1)} fusion(bf16[96,2,2048]{2,1,0:T(2,128)(2,1)S(1)} %gather.7, pred[96,2]{1,0:T(8,128)(4,1)S(1)} %copy.70, f32[96,2]{1,0:T(8,128)S(1)} %copy.65), kind=kLoop, calls=%fused_computation.12 | loop fusion | flops 1376256 | bytes 1573824 | tf_op jit(solution)/shard_map/reduce_sum | solution.py:272
  236.2 0.9 add_convert_fusion
  (51 shorter events, 1.9 us)
Async XLA Ops:
  6.5 52.8 %copy-start.1 = (f32[4]{0:T(128)S(1)}, f32[4]{0:T(128)}, u32[]{:S(2)}) copy-start(f32[4]{0:T(128)} %off_ref.1) | copy-start | bytes 52
  6.5 52.8 %all-gather.3.cloned.1.call-start = ((), (), s32[]{:S(2)}) async-start(), calls=%async_computation.3 | async-start | bytes 3379200 | tf_op jit(solution)/shard_map/all_gather | solution.py:225
  11.4 10.3 %collective-permute-start = (bf16[192,256]{1,0:T(8,128)(2,1)S(1)}, bf16[192,256]{1,0:T(8,128)(2,1)S(1)}, u32[]{:S(2)}, u32[]{:S(2)}) collective-permute-start(bf16[192,256]{1,0:T(8,128)(2,1)S(1)} %get-tuple-element.10), channel_id=1, source_target_pairs={{0,124},{4,120},{8,116},{12,112},{16,108},{20,104},{24,100},{28,96... | collective-permute-start | bytes 294920 | tf_op jit(solution)/shard_map/ppermute | solution.py:226
  59.3 1.9 copy-start
  61.3 57.1 %copy-start.3 = (s32[96,2]{0,1:T(2,128)S(1)}, s32[96,2]{0,1:T(2,128)}, u32[]{:S(2)}) copy-start(s32[96,2]{0,1:T(2,128)} %param.22) | copy-start | bytes 2308
  105.6 18.0 %copy-start.2 = (bf16[96,2048]{1,0:T(8,128)(2,1)S(1)}, bf16[96,2048]{1,0:T(8,128)(2,1)}, u32[]{:S(2)}) copy-start(bf16[96,2048]{1,0:T(8,128)(2,1)} %param.19) | copy-start | bytes 1179652
  105.6 8.1 %collective-permute-start.1 = (bf16[192,256]{1,0:T(8,128)(2,1)S(1)}, bf16[192,256]{1,0:T(8,128)(2,1)S(1)}, u32[]{:S(2)}, u32[]{:S(2)}) collective-permute-start(bf16[192,256]{1,0:T(8,128)(2,1)S(1)} %get-tuple-element.8), channel_id=1, source_target_pairs={{0,124},{4,120},{8,116},{12,112},{16,108},{20,104},{24,100},{28,96... | collective-permute-start | bytes 294920 | tf_op jit(solution)/shard_map/ppermute | solution.py:228
  114.4 9.2 %all-to-all-start = ((bf16[4,96,256]{2,1,0:T(8,128)(2,1)}), bf16[4,96,256]{2,1,0:T(8,128)(2,1)S(1)}, u32[]{:S(2)}, u32[]{:S(2)}) async-start(bf16[4,96,256]{2,1,0:T(8,128)(2,1)} %bitcast.6), calls=%async_computation | async-start | bytes 393216 | tf_op jit(solution)/shard_map/all_to_all | solution.py:229
  123.6 3.2 %copy-start.4 = (f32[2048]{0:T(1024)S(1)}, f32[2048]{0:T(1024)}, u32[]{:S(2)}) copy-start(f32[2048]{0:T(1024)} %param.21) | copy-start | bytes 24580
  191.8 5.4 %copy-start.5 = (f32[96,2]{0,1:T(2,128)S(1)}, f32[96,2]{0,1:T(2,128)}, u32[]{:S(2)}) copy-start(f32[96,2]{0,1:T(2,128)} %param.24) | copy-start | bytes 2308
  191.8 5.4 %copy-start.6 = (f32[96]{0:T(128)S(1)}, f32[96]{0:T(128)}, u32[]{:S(2)}) copy-start(f32[96]{0:T(128)} %param.23) | copy-start | bytes 1156
  191.8 35.5 %all-to-all-start.2 = ((bf16[128,3,2048]{2,1,0:T(4,128)(2,1)}), bf16[128,3,2048]{2,1,0:T(4,128)(2,1)}, u32[]{:S(2)}, u32[]{:S(2)}) async-start(bf16[128,3,2048]{2,1,0:T(4,128)(2,1)} %reshape.134), calls=%async_computation.2 | async-start | bytes 4194304 | tf_op jit(solution)/shard_map/all_to_all | solution.py:267
Sparse Core Ops, SparseCore 0:
  10.5 48.7 all-gather.2

commit v2 on v1

--- a/solution.py
+++ b/solution.py
@@ -1,4 +1,5 @@
 import functools
+
 import jax
 import jax.numpy as jnp
 from jax import lax
@@ -53,8 +54,8 @@
         c_hi = 1.4453125
         extra = jnp.where(row == 0, c_hi, jnp.where(row == 1, LOG2E - c_hi, jnp.where(row == 2, hi, jnp.where(row == 3, mid, jnp.where(row == 4, lo, 0.0)))))
         bottom = jnp.concatenate([extra, bottom[8:, :]], axis=0)
-        qt[0:128, s * COLS:(s + 1) * COLS] = top.astype(bf16)
-        qt[128:256, s * COLS:(s + 1) * COLS] = bottom.astype(bf16)
+        qt[s, 0:128, :] = top.astype(bf16)
+        qt[s, 128:256, :] = bottom.astype(bf16)
 
     sub = lax.broadcasted_iota(jnp.int32, (8, TILE), 0)
 
@@ -65,15 +66,13 @@
         e = e * jnp.where(sub >= 4, 1.0, pltpu.roll(e, 4, 0))
         return e
 
-    def tile(base, at, is_a, diag, slow):
-        col = pl.multiple_of(base + at, 128)
-        here = pl.ds(col, TILE)
-        z = jnp.dot(lk[...], qt[:, here], preferred_element_type=f32)
+    def tile(half, at, is_a, diag, slow, start):
+        here = slice(at, at + TILE)
+        z = jnp.dot(lk[...], qt[half, :, here], preferred_element_type=f32)
         if diag:
             lane = lax.broadcasted_iota(jnp.int32, (8, TILE), 1)
             query = (lane + at) % HALF + jnp.where(is_a, 0, HALF)
             limit = query - sub * SEG
-        start = carry[:, here]
         if slow:
             p = jnp.ones((8, TILE), f32)
             for r in reversed(range(SEG)):
@@ -82,7 +81,7 @@
                     beta = jnp.where(r < limit, beta, 0.0)
                 w = p * beta
                 p = p - w
-                wts[r * 8:(r + 1) * 8, :] = w
+                wts[r * 8:(r + 1) * 8, here] = w
             e = exclusive(p)
             total = e[0:1, :] * p[0:1, :]
             e = e * start
@@ -97,11 +96,11 @@
                         x = jnp.where(r < limit, x, 0.0)
                     w = x * f
                     f = f + w
-                    wts[r * 8:(r + 1) * 8, :] = w
+                    wts[r * 8:(r + 1) * 8, here] = w
                 fine = jnp.where(f < 1e36, 1.0, 0.0)
                 good = fine if good is None else jnp.minimum(good, fine)
                 ends.append(1.0 / f)
-            okay[:, 0:TILE] = jnp.minimum(okay[:, 0:TILE], good)
+            okay[:, here] = jnp.minimum(okay[:, here], good)
             p = ends[0] * ends[1] * ends[2]
             e = exclusive(p)
             total = e[0:1, :] * p[0:1, :]
@@ -109,13 +108,20 @@
             s2 = e * ends[2]
             s1 = s2 * ends[1]
             scales = [s1 * ends[0], s1, s2]
-        carry[:, here] = start * total
         both = [jnp.concatenate([s, s], axis=0) for s in scales]
         parts = []
         for r in range(0, SEG, 2):
-            parts.append((wts[r * 8:(r + 2) * 8, :] * both[r // CHUNK]).astype(bf16))
+            parts.append((wts[r * 8:(r + 2) * 8, here] * both[r // CHUNK]).astype(bf16))
         weight = jnp.concatenate(parts, axis=0)
-        acc[:, here] += jnp.dot(vt[...], weight, preferred_element_type=f32)
+        return start * total, jnp.dot(vt[...], weight, preferred_element_type=f32)
+
+    def tiles(half, is_a, diag, slow):
+        spots = range(0, COLS, TILE)
+        starts = [carry[half, :, at:at + TILE] for at in spots]
+        done = [tile(half, at, is_a, diag, slow, start) for at, start in zip(spots, starts)]
+        for at, (left, added) in zip(spots, done):
+            carry[half, :, at:at + TILE] = left
+            acc[half, :, at:at + TILE] += added
 
     def sweep(slow):
         acc[...] = jnp.zeros_like(acc)
@@ -124,7 +130,7 @@
         def step(s, c):
             is_a = s <= i
             block = jnp.where(is_a, i - s, n - s)
-            base = jnp.where(is_a, 0, COLS)
+            half = jnp.where(is_a, 0, 1)
             rows = kv_ref[block, 0:BLK, :]
             lk[:, 0:128] = rows
             wide = rows.astype(f32)
@@ -140,13 +146,11 @@
 
             @pl.when(edge)
             def _():
-                for at in range(0, COLS, TILE):
-                    tile(base, at, is_a, True, slow)
+                tiles(half, is_a, True, slow)
 
             @pl.when(jnp.logical_not(edge))
             def _():
-                for at in range(0, COLS, TILE):
-                    tile(base, at, is_a, False, slow)
+                tiles(half, is_a, False, slow)
             return c
 
         lax.fori_loop(0, n + 1, step, 0)
@@ -158,7 +162,7 @@
     def _():
         sweep(True)
 
-    stacked = jnp.concatenate([acc[:, 0:COLS], acc[:, COLS:2 * COLS]], axis=0).T
+    stacked = jnp.concatenate([acc[0], acc[1]], axis=0).T
     for s in range(2):
         heads = [stacked[h * HALF:(h + 1) * HALF, s * 64:(s + 1) * 64] for h in range(HEADS)]
         out_ref[s * HALF:(s + 1) * HALF, :] = jnp.concatenate(heads, axis=1).astype(bf16)
@@ -173,24 +177,130 @@
         in_specs=[sm, vm, vm, sm],
         out_specs=vm,
         scratch_shapes=[
-            pltpu.VMEM((256, 2 * COLS), jnp.bfloat16),
+            pltpu.VMEM((2, 256, COLS), jnp.bfloat16),
             pltpu.VMEM((BLK, 256), jnp.bfloat16),
             pltpu.VMEM((64, BLK), jnp.bfloat16),
-            pltpu.VMEM((64, 2 * COLS), jnp.float32),
-            pltpu.VMEM((8, 2 * COLS), jnp.float32),
-            pltpu.VMEM((8, TILE), jnp.float32),
-            pltpu.VMEM((BLK, TILE), jnp.float32),
+            pltpu.VMEM((2, 64, COLS), jnp.float32),
+            pltpu.VMEM((2, 8, COLS), jnp.float32),
+            pltpu.VMEM((8, COLS), jnp.float32),
+            pltpu.VMEM((BLK, COLS), jnp.float32),
         ],
         compiler_params=pltpu.CompilerParams(vmem_limit_bytes=40 * 1024 * 1024),
         name="attention",
     )(position, kv, q, offsets)
 
 
-def pack_block(key_rows, value_rows, key_logit):
-    both = jnp.concatenate([key_rows, value_rows], axis=1)
-    both = both.reshape(8, SEG, 128).transpose(1, 0, 2).reshape(BLK, 128)
-    logit = key_logit.reshape(8, SEG).T.reshape(3, 128)
-    return jnp.concatenate([both, logit, jnp.zeros((13, 128), jnp.bfloat16)], axis=0)
+ROWS = 400
+CUT = 192
+MESH = pl.DeviceIdType.MESH
+
+
+def gather_kernel(n, k_ref, v_ref, l_ref, q_ref, kv_ref, qs_ref, send, recv):
+    f32, bf16 = jnp.float32, jnp.bfloat16
+    me = lax.axis_index("sp")
+    z, y, core = me // 8, (me // 2) % 4, me % 2
+
+    def at(a, b, c):
+        dz, dy = a * c + b * (1 - c), a * (1 - c) + b * c
+        return ((z + dz + 4) % 4) * 8 + ((y + dy + 4) % 4) * 2 + c
+
+    other, mirror = me + 1 - 2 * core, n - 1 - me
+    near = [at(1, 0, core), at(3, 0, core)], [at(0, 1, core), at(0, 3, core)]
+    barrier = pltpu.get_barrier_semaphore()
+    for peer in near[0] + near[1] + [other, mirror]:
+        pl.semaphore_signal(barrier, inc=1, device_id={"sp": peer}, device_id_type=MESH)
+
+    spot = lax.broadcasted_iota(jnp.int32, (BLK, BLK), 0)
+    source = lax.broadcasted_iota(jnp.int32, (BLK, BLK), 1)
+    order = jnp.where(source == (spot % 8) * SEG + spot // 8, 1.0, 0.0).astype(bf16)
+    both = jnp.concatenate([k_ref[...], v_ref[...]], axis=1)
+    kv_ref[me, 0:BLK, :] = jnp.dot(order, both, preferred_element_type=f32).astype(bf16)
+    logit = jnp.broadcast_to(l_ref[...].astype(f32), (BLK, 128)).astype(bf16)
+    logit = jnp.dot(order, logit, preferred_element_type=f32)
+    row = lax.broadcasted_iota(jnp.int32, (16, 128), 0)
+    tail = jnp.zeros((16, 128), f32)
+    for j in range(3):
+        tail = jnp.where(row == j, logit[j * 128:(j + 1) * 128, :].T[0:16, :], tail)
+    kv_ref[me, BLK:ROWS, :] = tail.astype(bf16)
+    qs_ref[0:HALF, :] = q_ref[0:HALF, :]
+    pl.semaphore_wait(barrier, 6)
+
+    begun = []
+    parts = (slice(0, ROWS), slice(0, CUT), slice(CUT, ROWS))
+
+    def copy(index, slot, part, peer):
+        piece = kv_ref.at[slot, parts[part]]
+        return pltpu.make_async_remote_copy(
+            src_ref=piece, dst_ref=piece, send_sem=send.at[index], recv_sem=recv.at[index],
+            device_id={"sp": peer}, device_id_type=MESH)
+
+    def begin(index, slot, part, peer):
+        c = copy(index, slot, part, peer)
+        c.start()
+        begun.append(c)
+
+    def arrive(index, slot, part):
+        copy(index, slot, part, me).wait_recv()
+
+    around = (0, 3, 1, 2)
+
+    def spread(k, a):
+        slot = at(a, 0, core)
+        for d in range(2):
+            begin(4 + 4 * k + d, slot, 0, near[1][d])
+        begin(20 + k, slot, 0, other)
+
+    swap = pltpu.make_async_remote_copy(
+        src_ref=q_ref.at[HALF:BLK], dst_ref=qs_ref.at[HALF:BLK], send_sem=send.at[36], recv_sem=recv.at[36],
+        device_id={"sp": mirror}, device_id_type=MESH)
+    for d in range(2):
+        begin(d, me, 0, near[0][d])
+    spread(0, 0)
+    swap.start()
+    for d, a in ((0, 3), (1, 1)):
+        slot = at(a, 0, core)
+        arrive(d, slot, 0)
+        begin(2 + d, slot, 1 + d, near[0][d])
+        spread(1 + d, a)
+    for k, a in enumerate(around):
+        if k == 3:
+            slot = at(2, 0, core)
+            for d in range(2):
+                arrive(2 + d, slot, 1 + d)
+            spread(3, 2)
+        for d, b in ((0, 3), (1, 1)):
+            slot = at(a, b, core)
+            arrive(4 + 4 * k + d, slot, 0)
+            begin(6 + 4 * k + d, slot, 1 + d, near[1][d])
+            begin(24 + 4 * d + k, slot, 0, other)
+    for k, a in enumerate(around):
+        slot = at(a, 2, core)
+        for d in range(2):
+            arrive(6 + 4 * k + d, slot, 1 + d)
+        begin(32 + k, slot, 0, other)
+    for j, b in enumerate((0, 3, 1, 2)):
+        for k, a in enumerate(around):
+            arrive(20 + 4 * j + k, at(a, b, 1 - core), 0)
+    swap.wait_recv()
+    for c in begun:
+        c.wait_send()
+    swap.wait_send()
+
+
+def gather(n, k, v, logit, q):
+    vm = pl.BlockSpec(memory_space=pltpu.VMEM)
+    return pl.pallas_call(
+        functools.partial(gather_kernel, n),
+        out_shape=(
+            jax.ShapeDtypeStruct((n, ROWS, 128), jnp.bfloat16),
+            jax.ShapeDtypeStruct((BLK, HEADS * HEAD_DIM), jnp.bfloat16),
+        ),
+        in_specs=[vm] * 4,
+        out_specs=(vm, vm),
+        scratch_shapes=[pltpu.SemaphoreType.DMA((37,)), pltpu.SemaphoreType.DMA((37,))],
+        compiler_params=pltpu.CompilerParams(collective_id=0, has_side_effects=True, vmem_limit_bytes=24 * 1024 * 1024),
+        name="gather",
+    )(k, v, logit, q)
 
 
 def expert_apply(incoming, gate_one, up_one, down_one):
@@ -221,10 +331,8 @@
     n = lax.axis_size("sp")
     position = lax.axis_index("sp").astype(jnp.int32).reshape(1)
     mirror = [(a, n - 1 - a) for a in range(n)]
-    block = pack_block(key_rows, value_rows, key_logit)
-    kv = lax.all_gather(block, "sp", axis=0)
-    late = lax.ppermute(queries[HALF:], "sp", mirror)
-    halves = attention(n, position, kv, jnp.concatenate([queries[:HALF], late], axis=0), head_offset)
+    kv, chosen = gather(n, key_rows, value_rows, key_logit, queries)
+    halves = attention(n, position, kv, chosen, head_offset)
     attended = jnp.concatenate([halves[:HALF], lax.ppermute(halves[HALF:], "sp", mirror)], axis=0)
     token_heads = lax.all_to_all(attended, "tp", split_axis=0, concat_axis=1, tiled=True)
     mixed_rows = (

time: 245 us -> 256 us (1.045)
  blocking collectives: 36.4 us -> 84.1 us
  waiting for transfers between devices: 79.2 us -> 37.8 us
  Pallas kernels: 44.3 us -> 69.8 us
  between operations: 13.7 us -> 0.27 us
  starting transfers between devices: 19.2 us -> 13.3 us
    all_to_all x1, blocking collectives: 36.4 us -> 84.1 us  [on_device(): lax.all_to_all(outgoing, ('sp', 'tp'), split_axis=0, concat_axis=0, tiled...]
    all_gather x1 -> x0, waiting for transfers between devices: 37.7 us -> none  [on_device(): kv = lax.all_gather(block, 'sp', axis=0)]
    pallas_call x0 -> x1, Pallas kernels: none -> 25.7 us  [gather(): pl.pallas_call(functools.partial(gather_kernel, n), out_shape=(jax.ShapeD...]
    ppermute x1 -> x0, starting transfers between devices: 7.67 us -> none  [on_device(): late = lax.ppermute(queries[HALF:], 'sp', mirror)]
    ppermute x1, waiting for transfers between devices: 5.33 us -> 2.54 us  [on_device(): lax.ppermute(halves[HALF:], 'sp', mirror)]
  transfers between devices with their start and end apart: 5 -> 3, of which waited for: 5 -> 3; matrix products, arithmetic and copies ran while one was open for 1% -> 1% of each run, Pallas kernels for 0% -> 0%
where the time goes in v2:
time: 256 us; the launch traced here: 253 us
  blocking collectives  84.1 us (33%)
  Pallas kernels  69.8 us (27%)
  waiting for transfers between devices  37.8 us (15%)
  local copies, waits for them, and re-layouts  23.9 us (9%)
  matrix products  18.6 us (7%)
  starting transfers between devices  13.3 us (5%)
  other arithmetic  5.49 us (2%)
    all_to_all x1, blocking collectives, on_device(): lax.all_to_all(outgoing, ('sp', 'tp'), split_axis=0, concat_axis=0, tiled...  84.1 us
    pallas_call x1, Pallas kernels, attention(): pl.pallas_call(functools.partial(attention_kernel, n), out_shape=jax.Shap...  44.1 us
    all_to_all x1, waiting for transfers between devices, on_device(): lax.all_to_all(produced, ('sp', 'tp'), split_axis=0, concat_axis=0, tiled...  30 us
    pallas_call x1, Pallas kernels, gather(): pl.pallas_call(functools.partial(gather_kernel, n), out_shape=(jax.ShapeD...  25.7 us
    dot_general x1, matrix products, expert_apply(): jnp.dot(hidden, down_one, preferred_element_type=jnp.float32)  8.56 us
    all_to_all x1, waiting for transfers between devices, on_device(): lax.all_to_all(attended, 'tp', split_axis=0, concat_axis=1, tiled=True)  5.28 us
    reshape x1, local copies, waits for them, and re-layouts, expert_apply(): return produced.reshape(incoming.shape)  5.15 us
    dot_general x1, matrix products, expert_apply(): gate_act = jnp.dot(flat_rows, gate_one, preferred_element_type=jnp.float32)  5.13 us
  transfers between devices with their start and end apart: 3, of which 3 were waited for; matrix products, arithmetic and copies ran while one was open for 1% of the time, Pallas kernels for 0%

profile of v2, /device:TPU:1, one launch (start us, length us, event | category | flops | bytes accessed | tf_op | source)
XLA Modules:
  0.0 253.3 jit_solution(2257115536959434735)
XLA Ops:
  0.0 0.9 copy.49.k_ref
  0.9 0.9 copy.50.v_ref
  1.8 0.9 copy.51.l_ref
  2.7 0.9 copy-done
  3.6 25.7 %gather.11 = (bf16[32,400,128]{2,1,0:T(8,128)(2,1)S(1)}, bf16[384,256]{1,0:T(8,128)(2,1)S(1)}) custom-call(bf16[384,64]{1,0:T(8,128)(2,1)S(1)} %copy.49.k_ref, bf16[384,64]{1,0:T(8,128)(2,1)S(1)} %copy.50.v_ref, bf16[384,1]{1,0:T(8,128)(2,1)S(1)} %copy.51.l_ref, bf16[384,256]{1,0:T(8,128)(2,1)S(1)} %copy-done), custom_call_target="tpu_custom_call" | custom-call | tf_op jit(solution)/shard_map/gather/pallas_call | solution.py:292
  29.4 0.6 copy-done.1
  30.0 44.1 %attention.1 = bf16[384,256]{1,0:T(8,128)(2,1)S(1)} custom-call(s32[1]{0:T(128)} %bitcast.pos_ref, bf16[32,400,128]{2,1,0:T(8,128)(2,1)S(1)} %get-tuple-element.7.kv_ref, bf16[384,256]{1,0:T(8,128)(2,1)S(1)} %get-tuple-element.8.q_ref, f32[4]{0:T(128)S(1)} %copy-done.1), custom_call_target="tpu_custom_call" | custom-call | tf_op jit(solution)/shard_map/attention/pallas_call | solution.py:174
  74.2 4.4 %collective-permute-start = (bf16[192,256]{1,0:T(8,128)(2,1)S(1)}, bf16[192,256]{1,0:T(8,128)(2,1)S(1)}, u32[]{:S(2)}, u32[]{:S(2)}) collective-permute-start(bf16[192,256]{1,0:T(8,128)(2,1)S(1)} %get-tuple-element.12), channel_id=1, source_target_pairs={{0,124},{4,120},{8,116},{12,112},{16,108},{20,104},{24,100},{28,96... | collective-permute-start | bytes 294920 | tf_op jit(solution)/shard_map/ppermute | solution.py:336
  78.6 0.1 reshape.113
  78.9 0.1 fusion.18
  79.1 0.2 fusion.20
  79.3 0.1 sub.9
  79.5 2.5 %collective-permute-done = bf16[192,256]{1,0:T(8,128)(2,1)S(1)} collective-permute-done((bf16[192,256]{1,0:T(8,128)(2,1)S(1)}, bf16[192,256]{1,0:T(8,128)(2,1)S(1)}, u32[]{:S(2)}, u32[]{:S(2)}) %collective-permute-start) | collective-permute-done | bytes 98336 | tf_op jit(solution)/shard_map/ppermute | solution.py:336
  82.1 0.7 pad_maximum_fusion
  82.8 4.0 %all-to-all-start = ((bf16[4,96,256]{2,1,0:T(8,128)(2,1)}), bf16[4,96,256]{2,1,0:T(8,128)(2,1)S(1)}, u32[]{:S(2)}, u32[]{:S(2)}) async-start(bf16[4,96,256]{2,1,0:T(8,128)(2,1)} %bitcast.1), calls=%async_computation | async-start | bytes 393216 | tf_op jit(solution)/shard_map/all_to_all | solution.py:337
  86.9 5.3 %all-to-all-done = bf16[4,96,256]{2,1,0:T(8,128)(2,1)S(1)} async-done(((bf16[4,96,256]{2,1,0:T(8,128)(2,1)}), bf16[4,96,256]{2,1,0:T(8,128)(2,1)S(1)}, u32[]{:S(2)}, u32[]{:S(2)}) %all-to-all-start) | async-done | bytes 196640 | tf_op jit(solution)/shard_map/all_to_all | solution.py:337
  92.2 3.1 %multiply_reduce_fusion.1 = (f32[96]{0:T(128)S(1)}, f32[96,2048]{1,0:T(8,128)S(1)}) fusion(bf16[96,1024]{1,0:T(8,128)(2,1)S(1)} %bitcast.35, bf16[1024,2048]{1,0:T(8,128)(2,1)} %param.20, bf16[96,2048]{1,0:T(8,128)(2,1)S(1)} %copy-done.2), kind=kOutput, calls=%fused_computation.18 | convolution fusion | flops 403832736 | bytes 5570944 | tf_op jit(solution)/shard_map/dot_general | solution.py:340
  95.4 1.8 convolution_convert_fusion
  97.2 4.0 %reshape.116 = bf16[128,3,2048]{2,1,0:T(4,128)(2,1)S(1)} reshape(bf16[384,2048]{1,0:T(8,128)(2,1)} %convolution_convert_fusion) | data formatting | bytes 3145728 | tf_op jit(solution)/shard_map/reshape | solution.py:368
  101.2 84.1 %all_to_all.29 = bf16[128,3,2048]{2,1,0:T(4,128)(2,1)} all-to-all(bf16[128,3,2048]{2,1,0:T(4,128)(2,1)S(1)} %reshape.116), channel_id=1, replica_groups=mesh['sp'=32,'tp'=4] {'sp','tp'}, dimensions={0} | all-to-all | bytes 3145728 | tf_op jit(solution)/shard_map/all_to_all | solution.py:370
  185.3 3.9 %reshape.117 = bf16[384,2048]{1,0:T(8,128)(2,1)S(1)} reshape(bf16[128,3,2048]{2,1,0:T(4,128)(2,1)} %all_to_all.29) | data formatting | bytes 3145728 | tf_op jit(solution)/shard_map/reshape | solution.py:307
  189.2 5.1 %fusion.4 = f32[384,1024]{1,0:T(8,128)} fusion(bf16[384,2048]{1,0:T(8,128)(2,1)S(1)} %reshape.117, bf16[1,2048,1024]{2,1,0:T(8,128)(2,1)} %param.25), kind=kOutput, calls=%fused_computation.5 | convolution fusion | flops 1610612736 | bytes 7340032 | tf_op jit(solution)/shard_map/dot_general | solution.py:308
  194.4 8.6 %fusion.6 = bf16[384,2048]{1,0:T(8,128)(2,1)} fusion(bf16[1,1024,2048]{2,1,0:T(8,128)(2,1)} %param.27, f32[384,1024]{1,0:T(8,128)} %fusion.4, bf16[384,2048]{1,0:T(8,128)(2,1)S(1)} %reshape.117, bf16[1,2048,1024]{2,1,0:T(8,128)(2,1)} %param.26), kind=kOutput, calls=%fused_computation.7 | convolution fusion | flops 3224371200 | bytes 13107200 | tf_op jit(solution)/shard_map/dot_general | solution.py:311
  202.9 5.1 %reshape.118 = bf16[128,3,2048]{2,1,0:T(4,128)(2,1)} reshape(bf16[384,2048]{1,0:T(8,128)(2,1)} %fusion.6) | data formatting | bytes 3145728 | tf_op jit(solution)/shard_map/reshape | solution.py:312
  208.1 5.0 %all-to-all-start.2 = ((bf16[128,3,2048]{2,1,0:T(4,128)(2,1)}), bf16[128,3,2048]{2,1,0:T(4,128)(2,1)}, u32[]{:S(2)}, u32[]{:S(2)}) async-start(bf16[128,3,2048]{2,1,0:T(4,128)(2,1)} %reshape.118), calls=%async_computation.2 | async-start | bytes 4194304 | tf_op jit(solution)/shard_map/all_to_all | solution.py:375
  213.2 0.1 mul.81
  213.6 30.0 %all-to-all-done.2 = bf16[128,3,2048]{2,1,0:T(4,128)(2,1)} async-done(((bf16[128,3,2048]{2,1,0:T(4,128)(2,1)}), bf16[128,3,2048]{2,1,0:T(4,128)(2,1)}, u32[]{:S(2)}, u32[]{:S(2)}) %all-to-all-start.2) | async-done | bytes 1572896 | tf_op jit(solution)/shard_map/all_to_all | solution.py:375
  243.6 3.9 %reshape.119 = bf16[384,2048]{1,0:T(8,128)(2,1)S(1)} reshape(bf16[128,3,2048]{2,1,0:T(4,128)(2,1)} %all-to-all-done.2) | data formatting | bytes 3145728 | tf_op jit(solution)/shard_map/reshape | solution.py:376
  247.5 1.1 gather_fusion
  248.7 0.5 gather.8
  249.2 3.3 %multiply_reduce_fusion = f32[96,2048]{1,0:T(8,128)S(1)} fusion(bf16[96,2,2048]{2,1,0:T(2,128)(2,1)S(1)} %gather.8, pred[96,2]{1,0:T(8,128)(4,1)S(1)} %copy.58, f32[96,2]{1,0:T(8,128)S(1)} %copy.53), kind=kLoop, calls=%fused_computation.12 | loop fusion | flops 1376256 | bytes 1573824 | tf_op jit(solution)/shard_map/reduce_sum | solution.py:380
  252.5 0.9 add_convert_fusion
  (37 shorter events, 0.9 us)
Async XLA Ops:
  2.7 0.9 copy-start
  29.3 0.7 copy-start.1
  30.0 48.5 %copy-start.3 = (s32[96,2]{0,1:T(2,128)S(1)}, s32[96,2]{0,1:T(2,128)}, u32[]{:S(2)}) copy-start(s32[96,2]{0,1:T(2,128)} %param.22) | copy-start | bytes 2308
  74.1 18.1 %copy-start.2 = (bf16[96,2048]{1,0:T(8,128)(2,1)S(1)}, bf16[96,2048]{1,0:T(8,128)(2,1)}, u32[]{:S(2)}) copy-start(bf16[96,2048]{1,0:T(8,128)(2,1)} %param.19) | copy-start | bytes 1179652
  74.2 7.9 %collective-permute-start = (bf16[192,256]{1,0:T(8,128)(2,1)S(1)}, bf16[192,256]{1,0:T(8,128)(2,1)S(1)}, u32[]{:S(2)}, u32[]{:S(2)}) collective-permute-start(bf16[192,256]{1,0:T(8,128)(2,1)S(1)} %get-tuple-element.12), channel_id=1, source_target_pairs={{0,124},{4,120},{8,116},{12,112},{16,108},{20,104},{24,100},{28,96... | collective-permute-start | bytes 294920 | tf_op jit(solution)/shard_map/ppermute | solution.py:336
  82.8 9.4 %all-to-all-start = ((bf16[4,96,256]{2,1,0:T(8,128)(2,1)}), bf16[4,96,256]{2,1,0:T(8,128)(2,1)S(1)}, u32[]{:S(2)}, u32[]{:S(2)}) async-start(bf16[4,96,256]{2,1,0:T(8,128)(2,1)} %bitcast.1), calls=%async_computation | async-start | bytes 393216 | tf_op jit(solution)/shard_map/all_to_all | solution.py:337
  92.2 3.2 %copy-start.4 = (f32[2048]{0:T(1024)S(1)}, f32[2048]{0:T(1024)}, u32[]{:S(2)}) copy-start(f32[2048]{0:T(1024)} %param.21) | copy-start | bytes 24580
  208.1 5.4 %copy-start.5 = (f32[96,2]{0,1:T(2,128)S(1)}, f32[96,2]{0,1:T(2,128)}, u32[]{:S(2)}) copy-start(f32[96,2]{0,1:T(2,128)} %param.24) | copy-start | bytes 2308
  208.1 5.4 %copy-start.6 = (f32[96]{0:T(128)S(1)}, f32[96]{0:T(128)}, u32[]{:S(2)}) copy-start(f32[96]{0:T(128)} %param.23) | copy-start | bytes 1156
  208.1 35.5 %all-to-all-start.2 = ((bf16[128,3,2048]{2,1,0:T(4,128)(2,1)}), bf16[128,3,2048]{2,1,0:T(4,128)(2,1)}, u32[]{:S(2)}, u32[]{:S(2)}) async-start(bf16[128,3,2048]{2,1,0:T(4,128)(2,1)} %reshape.118), calls=%async_computation.2 | async-start | bytes 4194304 | tf_op jit(solution)/shard_map/all_to_all | solution.py:375
